TPU v7x, 32 devices: a whole 2x2x4 slice. The times are simulated.
32 devices in a mesh: sp: 8 (over z, y), tp: 4 (over x, core).
Axes of the slice: x: 2, y: 2, z: 4, core: 2. Of those that a mesh axis runs over, the one named last changes fastest.
Arguments:
- residual_in: bfloat16 [6144, 2048], P('sp', 'tp'), may hold values from -11 to 11
- queries: bfloat16 [6144, 1024], P('sp', 'tp'), may hold values from -6 to 6
- keys: bfloat16 [6144, 256], P('sp'), may hold values from -6 to 6
- values: bfloat16 [6144, 256], P('sp'), may hold values from -6 to 6
- query_gain: float32 [128], replicated, may hold values from 1.5 to 5
- key_norm_gain: float32 [128], replicated, may hold values from 1.5 to 5
- out_weight: bfloat16 [1024, 2048], P('tp'), may hold values from -0.1875 to 0.1875
- mlp_gain: float32 [2048], replicated, may hold values from 0.1 to 1.9
- gate_weight: bfloat16 [2048, 5632], P('sp', 'tp'), may hold values from -0.125 to 0.125
- up_weight: bfloat16 [2048, 5632], P('sp', 'tp'), may hold values from -0.125 to 0.125
- down_weight: bfloat16 [5632, 2048], P('tp', 'sp'), may hold values from -0.15625 to 0.15625
Outputs:
- layer_out: bfloat16 [6144, 2048], P('sp', 'tp')
All inputs are finite; a program needn't handle non-finite values.
Results may differ from a plain program's by a relative error of at most 0.012.
The roundings to bfloat16 on the way count: a program that leaves them out, or rounds other values in their place, can miss the bound.
Values may be sent and summed in bfloat16 or wider, within the bound.
A program may use at most 64 MiB of HBM per device.

v0:
```python
import jax
import jax.numpy as jnp
from jax import lax
from jax.sharding import PartitionSpec as P

D = 2048
HEAD_SIZE = 128
QUERY_HEADS = 8
KEY_VALUE_HEADS = 2
GRID = 64


eps = 1e-06
rotary_base = 10000.0


def apply_rotary(vectors, grid_positions):
    half_size = vectors.shape[-1] // 2
    frequency = rotary_base ** (-jnp.arange(0, half_size, 2, dtype=jnp.float32) / half_size)
    grid_row = (grid_positions // GRID).astype(jnp.float32)
    grid_col = (grid_positions % GRID).astype(jnp.float32)
    angles = jnp.concatenate(
        [grid_row[:, None] * frequency, grid_col[:, None] * frequency], axis=-1
    )[:, None, :]
    cosine_table = jnp.cos(angles)
    sine_table = jnp.sin(angles)
    first_half = vectors[..., :half_size]
    second_half = vectors[..., half_size:]
    return jnp.concatenate(
        [
            first_half * cosine_table - second_half * sine_table,
            first_half * sine_table + second_half * cosine_table,
        ],
        axis=-1,
    )


def per_head_norm(vectors, gain):
    return vectors * lax.rsqrt(jnp.mean(vectors * vectors, axis=-1, keepdims=True) + eps) * gain


def on_device(
    residual_in,
    queries,
    keys,
    values,
    query_gain,
    key_norm_gain,
    out_weight,
    mlp_gain,
    gate_weight,
    up_weight,
    down_weight,
):
    local_rows = residual_in.shape[0]
    local_heads = queries.shape[1] // HEAD_SIZE
    queries_per_group = QUERY_HEADS // KEY_VALUE_HEADS
    tp_index = lax.axis_index("tp")
    grid_positions = lax.axis_index("sp") * local_rows + jnp.arange(local_rows, dtype=jnp.int32)
    query_rows = apply_rotary(
        per_head_norm(
            queries.astype(jnp.float32).reshape(local_rows, local_heads, HEAD_SIZE), query_gain
        ),
        grid_positions,
    ).astype(jnp.bfloat16)
    query_matrix = jnp.transpose(query_rows, (1, 0, 2)).reshape(local_heads * local_rows, HEAD_SIZE)
    shared = tp_index * local_heads // queries_per_group
    own_keys = lax.dynamic_slice_in_dim(keys, shared * HEAD_SIZE, HEAD_SIZE, 1)
    own_values = lax.dynamic_slice_in_dim(values, shared * HEAD_SIZE, HEAD_SIZE, 1)
    key_matrix = apply_rotary(
        per_head_norm(own_keys.astype(jnp.float32)[:, None, :], key_norm_gain), grid_positions
    )[:, 0, :].astype(jnp.bfloat16)
    score_scale = HEAD_SIZE ** (-0.5)
    query_count = local_heads * local_rows
    start_state = (
        jnp.full((query_count,), -1e30, jnp.float32),
        jnp.zeros((query_count,), jnp.float32),
        jnp.zeros((query_count, HEAD_SIZE), jnp.float32),
    )
    key_piece = lax.all_gather(key_matrix, "sp", axis=0, tiled=True)
    value_piece = lax.all_gather(own_values, "sp", axis=0, tiled=True)
    piece_rows = key_piece.shape[0]
    block_count = -(-piece_rows // 2048)
    while piece_rows % block_count:
        block_count += 1
    block_width = piece_rows // block_count

    def one_block(block_index, state_inner):
        running_max, running_sum, weighted = state_inner
        block_keys = lax.dynamic_slice_in_dim(key_piece, block_index * block_width, block_width, 0)
        block_values = lax.dynamic_slice_in_dim(
            value_piece, block_index * block_width, block_width, 0
        )
        scores = (
            jnp.dot(query_matrix, block_keys.T, preferred_element_type=jnp.float32) * score_scale
        )
        new_max = jnp.maximum(running_max, jnp.max(scores, axis=1))
        factor = jnp.exp(running_max - new_max)
        weights = jnp.exp(scores - new_max[:, None])
        running_sum = running_sum * factor + jnp.sum(weights, axis=1)
        weighted = weighted * factor[:, None] + jnp.dot(
            weights.astype(jnp.bfloat16), block_values, preferred_element_type=jnp.float32
        )
        return (new_max, running_sum, weighted)

    running_max, running_sum, weighted = lax.fori_loop(0, block_count, one_block, start_state)
    attended = (weighted / running_sum[:, None]).astype(jnp.bfloat16)
    attended = jnp.transpose(
        attended.reshape(local_heads, local_rows, HEAD_SIZE), (1, 0, 2)
    ).reshape(local_rows, local_heads * HEAD_SIZE)
    own_width = residual_in.shape[1]
    projected = jnp.dot(attended, out_weight, preferred_element_type=jnp.float32).astype(
        jnp.bfloat16
    )
    share = lax.psum_scatter(projected, "tp", scatter_dimension=1, tiled=True).astype(jnp.float32)
    residual_mid = residual_in.astype(jnp.float32) + share
    squares = lax.psum(jnp.sum(residual_mid * residual_mid, axis=1), "tp")
    gain_own = lax.dynamic_slice_in_dim(mlp_gain, tp_index * own_width, own_width, 0)
    normed_own = (residual_mid * lax.rsqrt(squares / D + eps)[:, None] * gain_own).astype(
        jnp.bfloat16
    )
    normed = lax.all_gather(normed_own, "tp", axis=1, tiled=True)
    gate_out = jnp.dot(
        normed,
        lax.all_gather(gate_weight, "sp", axis=0, tiled=True),
        preferred_element_type=jnp.float32,
    )
    up_out = jnp.dot(
        normed,
        lax.all_gather(up_weight, "sp", axis=0, tiled=True),
        preferred_element_type=jnp.float32,
    )
    hidden = (jax.nn.silu(gate_out) * up_out).astype(jnp.bfloat16)
    down_terms = jnp.dot(
        hidden,
        lax.all_gather(down_weight, "sp", axis=1, tiled=True),
        preferred_element_type=jnp.float32,
    )
    down_share = lax.psum_scatter(
        down_terms.astype(jnp.bfloat16), "tp", scatter_dimension=1, tiled=True
    ).astype(jnp.float32)
    return (residual_mid + 0.5 * down_share).astype(jnp.bfloat16)


def solution(mesh):
    in_specs = (
        P("sp", "tp"),
        P("sp", "tp"),
        P("sp", None),
        P("sp", None),
        P(),
        P(),
        P("tp", None),
        P(),
        P("sp", "tp"),
        P("sp", "tp"),
        P("tp", "sp"),
    )
    out_specs = P("sp", "tp")
    return jax.shard_map(
        on_device, mesh=mesh, in_specs=in_specs, out_specs=out_specs, check_vma=False
    )
```

profile of v0, /device:TPU:24, one launch (start us, length us, event | category | flops | bytes accessed | tf_op | source)
XLA Modules:
  0.0 571.3 jit_solution(10254005252952721331)
XLA Ops:
  9.2 1.8 subtract_convert_fusion.1
  12.8 1.4 reshape.236
  14.1 1.7 fusion.18
  17.8 1.4 subtract_convert_fusion
  20.3 35.2 %all-gather.18.cloned.1.call-done = bf16[6144,1,128]{2,0,1:T(8,128)(2,1)} async-done(((bf16[768,1,128]{2,0,1:T(8,128)(2,1)}), bf16[6144,1,128]{2,0,1:T(8,128)(2,1)}) %all-gather.18.cloned.1.call-update) | async-done | bytes 1572880 | tf_op jit(solution)/shard_map/all_gather | solution.py:80
  55.6 44.8 %all-gather.8.cloned.1.call-done = bf16[6144,128]{1,0:T(8,128)(2,1)} async-done(((bf16[768,128]{1,0:T(8,128)(2,1)}), bf16[6144,128]{1,0:T(8,128)(2,1)}) %all-gather.8.cloned.1.call-update) | async-done | bytes 1572880 | tf_op jit(solution)/shard_map/all_gather | solution.py:81
  100.3 57.6 %while.18 = (s32[]{:T(128)}, f32[1536]{0:T(1024)S(1)}, f32[1536]{0:T(1024)S(1)}, f32[1536,128]{1,0:T(8,128)S(1)}, bf16[6144,128]{1,0:T(8,128)(2,1)}, /*index=5*/...) while((s32[]{:T(128)}, f32[1536]{0:T(1024)S(1)}, ...), condition=%wide.region_5.6_spmd.clone, body=%wide.region_2.5_spmd.clone.sunk | while | flops 1636376064 | bytes 91193544 | solution.py:106
  100.3 7.4 %multiply_reduce_fusion.4 = (f32[1536]{0:T(1024)S(1)}, f32[2048,1536]{1,0:T(8,128)}) fusion(bf16[1536,128]{1,0:T(8,128)(2,1)S(1)} %get-tuple-element.266, bf16[6144,128]{1,0:T(8,128)(2,1)} %get-tuple-element.265, s32[]{:T(128)S(6)} %select_n.55), kind=kOutput, calls=%fused_computation.1.clone.1 | convolution fusion | flops 811596288 | bytes 13506564 | tf_op jit(solution)/shard_map/while/body/eval_jaxpr/dot_general | solution.py:95
  107.7 6.8 %fusion.49 = f32[1536]{0:T(1024)S(1)} fusion(f32[2048,1536]{1,0:T(8,128)} %get-tuple-element.236, f32[1536]{0:T(1024)S(1)} %select_maximum_fusion.2), kind=kLoop, calls=%fused_computation.3.clone.1 | loop fusion | flops 9435648 | bytes 12595200 | tf_op jit(solution)/shard_map/while/body/eval_jaxpr/reduce_sum | solution.py:100
  114.5 1.3 copy-done.1
  115.8 3.6 fusion.51
  119.5 7.4 %multiply_reduce_fusion.4 = (f32[1536]{0:T(1024)S(1)}, f32[2048,1536]{1,0:T(8,128)}) fusion(bf16[1536,128]{1,0:T(8,128)(2,1)S(1)} %get-tuple-element.266, bf16[6144,128]{1,0:T(8,128)(2,1)} %get-tuple-element.265, s32[]{:T(128)S(6)} %select_n.55), kind=kOutput, calls=%fused_computation.1.clone.1 | convolution fusion | flops 811596288 | bytes 13506564 | tf_op jit(solution)/shard_map/while/body/eval_jaxpr/dot_general | solution.py:95
  126.9 6.8 %fusion.49 = f32[1536]{0:T(1024)S(1)} fusion(f32[2048,1536]{1,0:T(8,128)} %get-tuple-element.236, f32[1536]{0:T(1024)S(1)} %select_maximum_fusion.2), kind=kLoop, calls=%fused_computation.3.clone.1 | loop fusion | flops 9435648 | bytes 12595200 | tf_op jit(solution)/shard_map/while/body/eval_jaxpr/reduce_sum | solution.py:100
  133.7 1.3 copy-done.1
  135.0 3.6 fusion.51
  138.7 7.4 %multiply_reduce_fusion.4 = (f32[1536]{0:T(1024)S(1)}, f32[2048,1536]{1,0:T(8,128)}) fusion(bf16[1536,128]{1,0:T(8,128)(2,1)S(1)} %get-tuple-element.266, bf16[6144,128]{1,0:T(8,128)(2,1)} %get-tuple-element.265, s32[]{:T(128)S(6)} %select_n.55), kind=kOutput, calls=%fused_computation.1.clone.1 | convolution fusion | flops 811596288 | bytes 13506564 | tf_op jit(solution)/shard_map/while/body/eval_jaxpr/dot_general | solution.py:95
  146.1 6.8 %fusion.49 = f32[1536]{0:T(1024)S(1)} fusion(f32[2048,1536]{1,0:T(8,128)} %get-tuple-element.236, f32[1536]{0:T(1024)S(1)} %select_maximum_fusion.2), kind=kLoop, calls=%fused_computation.3.clone.1 | loop fusion | flops 9435648 | bytes 12595200 | tf_op jit(solution)/shard_map/while/body/eval_jaxpr/reduce_sum | solution.py:100
  152.9 1.3 copy-done.1
  154.2 3.6 fusion.51
  158.4 2.7 convolution_convert_fusion
  162.7 36.3 %reduce-scatter.3.cloned.1.call-done = bf16[768,512]{1,0:T(8,128)(2,1)} async-done(((bf16[768,2048]{1,0:T(8,128)(2,1)}), bf16[768,512]{1,0:T(8,128)(2,1)}) %reduce-scatter.3.cloned.1.call-update) | async-done | bytes 786448 | tf_op jit(solution)/shard_map/reduce_scatter | solution.py:115
  199.0 1.5 multiply_reduce_fusion.1
  200.5 6.0 %psum.7 = f32[768]{0:T(1024)S(1)} all-reduce(f32[768]{0:T(1024)S(1)} %multiply_reduce_fusion.1), channel_id=1, replica_groups=mesh['sp'=8,'tp'=4] {'tp'}, use_global_device_ids=true, to_apply=%region_8.9 | all-reduce | flops 768 | bytes 6144 | tf_op jit(solution)/shard_map/psum | solution.py:117
  206.4 2.3 multiply_convert_fusion.1
  210.2 81.3 %all-gather.12.cloned.1.call-done = bf16[2048,1408]{1,0:T(8,128)(2,1)} async-done(((bf16[256,1408]{1,0:T(8,128)(2,1)}), bf16[2048,1408]{1,0:T(8,128)(2,1)}) %all-gather.12.cloned.1.call-update) | async-done | bytes 5767184 | tf_op jit(solution)/shard_map/all_gather | solution.py:125
  291.5 30.0 %all-gather.10.cloned.1.call-done = bf16[768,2048]{1,0:T(8,128)(2,1)} async-done(((bf16[768,512]{1,0:T(8,128)(2,1)}), bf16[768,2048]{1,0:T(8,128)(2,1)}) %all-gather.10.cloned.1.call-update) | async-done | bytes 3145744 | tf_op jit(solution)/shard_map/all_gather | solution.py:122
  321.5 9.7 %fusion.31 = f32[768,1408]{1,0:T(8,128)} fusion(bf16[768,2048]{1,0:T(8,128)(2,1)} %all-gather.10.cloned.1.call-done, bf16[2048,1408]{1,0:T(8,128)(2,1)} %all-gather.12.cloned.1.call-done), kind=kOutput, calls=%fused_computation.68 | convolution fusion | flops 4429185024 | bytes 13238272 | tf_op jit(solution)/shard_map/dot_general | solution.py:123
  331.2 82.8 %all-gather.14.cloned.1.call-done = bf16[2048,1408]{1,0:T(8,128)(2,1)} async-done(((bf16[256,1408]{1,0:T(8,128)(2,1)}), bf16[2048,1408]{1,0:T(8,128)(2,1)}) %all-gather.14.cloned.1.call-update) | async-done | bytes 5767184 | tf_op jit(solution)/shard_map/all_gather | solution.py:130
  414.0 93.4 %all-gather.16.cloned.1.call-done = bf16[1408,2048]{1,0:T(8,128)(2,1)} async-done(((bf16[1408,256]{1,0:T(8,128)(2,1)}), bf16[1408,2048]{1,0:T(8,128)(2,1)}) %all-gather.16.cloned.1.call-update) | async-done | bytes 5767184 | tf_op jit(solution)/shard_map/all_gather | solution.py:136
  507.4 16.8 %convolution_convert_fusion.1 = bf16[768,2048]{1,0:T(8,128)(2,1)} fusion(bf16[1408,2048]{1,0:T(8,128)(2,1)} %all-gather.16.cloned.1.call-done, f32[768,1408]{1,0:T(8,128)} %fusion.31, bf16[768,2048]{1,0:T(8,128)(2,1)} %all-gather.10.cloned.1.call-done, bf16[2048,1408]{1,0:T(8,128)(2,1)} %all-gather.14.cloned.1.call-done), kind=kOutput, calls=%fused_computation.19 | convolution fusion | flops 8866430976 | bytes 22151168 | tf_op jit(solution)/shard_map/dot_general | solution.py:134
  524.2 38.0 %reduce-scatter.5.cloned.1.call-done = bf16[768,512]{1,0:T(8,128)(2,1)} async-done(((bf16[768,2048]{1,0:T(8,128)(2,1)}), bf16[768,512]{1,0:T(8,128)(2,1)}) %reduce-scatter.5.cloned.1.call-update) | async-done | bytes 786448 | tf_op jit(solution)/shard_map/reduce_scatter | solution.py:139
  562.1 2.3 add_convert_fusion
  (58 shorter events, 10.8 us)
Async XLA Ops:
  6.5 151.8 %copy-start = (bf16[256,2048]{1,0:T(8,128)(2,1)S(1)}, bf16[256,2048]{1,0:T(8,128)(2,1)}, u32[]{:S(2)}) copy-start(bf16[256,2048]{1,0:T(8,128)(2,1)} %param.19) | copy-start | bytes 3145732
  6.5 5.4 copy-start.4
  6.5 49.0 %all-gather.18.cloned.1.call-start = ((), (), s32[]{:S(2)}) async-start(), calls=%async_computation.9 | async-start | bytes 1769472 | tf_op jit(solution)/shard_map/all_gather | solution.py:80
  9.2 7.5 %copy-start.5 = (f32[128]{0:T(128)S(1)}, f32[128]{0:T(128)}, u32[]{:S(2)}) copy-start(f32[128]{0:T(128)} %param.17) | copy-start | bytes 1540
  11.9 88.4 %all-gather.8.cloned.1.call-start = ((), (), s32[]{:S(2)}) async-start(), calls=%async_computation.2 | async-start | bytes 1769472 | tf_op jit(solution)/shard_map/all_gather | solution.py:81
  12.7 186.3 %reduce-scatter.3.cloned.1.call-start = ((), (), s32[]{:S(2)}) async-start(), calls=%async_computation.3 | async-start | bytes 3932160 | tf_op jit(solution)/shard_map/reduce_scatter | solution.py:115
  107.7 8.2 %copy-start.1 = (f32[2048,1536]{1,0:T(8,128)S(1)}, f32[2048,1536]{1,0:T(8,128)}, u32[]{:S(2)}) copy-start(f32[2048,1536]{1,0:T(8,128)} %get-tuple-element.236) | copy-start | bytes 37748740 | tf_op jit(solution)/shard_map/while
  126.9 8.2 %copy-start.1 = (f32[2048,1536]{1,0:T(8,128)S(1)}, f32[2048,1536]{1,0:T(8,128)}, u32[]{:S(2)}) copy-start(f32[2048,1536]{1,0:T(8,128)} %get-tuple-element.236) | copy-start | bytes 37748740 | tf_op jit(solution)/shard_map/while
  146.1 8.2 %copy-start.1 = (f32[2048,1536]{1,0:T(8,128)S(1)}, f32[2048,1536]{1,0:T(8,128)}, u32[]{:S(2)}) copy-start(f32[2048,1536]{1,0:T(8,128)} %get-tuple-element.236) | copy-start | bytes 37748740 | tf_op jit(solution)/shard_map/while
  158.4 40.6 %copy-start.2 = (bf16[768,512]{1,0:T(8,128)(2,1)S(1)}, bf16[768,512]{1,0:T(8,128)(2,1)}, u32[]{:S(2)}) copy-start(bf16[768,512]{1,0:T(8,128)(2,1)} %param.13) | copy-start | bytes 2359300
  161.1 130.4 %all-gather.12.cloned.1.call-start = ((), (), s32[]{:S(2)}) async-start(), calls=%async_computation.5 | async-start | bytes 6488064 | tf_op jit(solution)/shard_map/all_gather | solution.py:125
  161.7 159.8 %all-gather.10.cloned.1.call-start = ((), (), s32[]{:S(2)}) async-start(), calls=%async_computation.4 | async-start | bytes 3932160 | tf_op jit(solution)/shard_map/all_gather | solution.py:122
  208.8 205.2 %all-gather.14.cloned.1.call-start = ((), (), s32[]{:S(2)}) async-start(), calls=%async_computation.6 | async-start | bytes 6488064 | tf_op jit(solution)/shard_map/all_gather | solution.py:130
  209.4 298.0 %all-gather.16.cloned.1.call-start = ((), (), s32[]{:S(2)}) async-start(), calls=%async_computation.7 | async-start | bytes 6488064 | tf_op jit(solution)/shard_map/all_gather | solution.py:136
  210.1 352.0 %reduce-scatter.5.cloned.1.call-start = ((), (), s32[]{:S(2)}) async-start(), calls=%async_computation.8 | async-start | bytes 3932160 | tf_op jit(solution)/shard_map/reduce_scatter | solution.py:139
  331.2 230.9 %copy-start.3 = (bf16[768,512]{1,0:T(8,128)(2,1)S(1)}, bf16[768,512]{1,0:T(8,128)(2,1)}, u32[]{:S(2)}) copy-start(bf16[768,512]{1,0:T(8,128)(2,1)} %reduce-scatter.3.cloned.1.call-done) | copy-start | bytes 2359300
Sparse Core Ops, SparseCore 0:
  12.0 43.5 all-gather.17
  57.7 42.5 all-gather.7
  161.2 37.7 reduce-scatter.2
  201.0 90.4 all-gather.11
  292.9 28.5 all-gather.9
  323.5 90.4 all-gather.13
  416.1 91.2 all-gather.15
  524.3 37.7 reduce-scatter.4
where the time goes:
time: 574 us; the launch traced here: 571 us
  waiting for transfers between devices  444 us (77%)
  matrix products  62.2 us (11%)
  other arithmetic  38.3 us (7%)
  between operations  13.7 us (2%)
  local copies, waits for them, and re-layouts  7.03 us (1%)
  blocking collectives  5.99 us (1%)
    all_gather x1, waiting for transfers between devices, on_device(): lax.all_gather(down_weight, 'sp', axis=1, tiled=True)  93.4 us
    all_gather x1, waiting for transfers between devices, on_device(): lax.all_gather(up_weight, 'sp', axis=0, tiled=True)  82.8 us
    all_gather x1, waiting for transfers between devices, on_device(): lax.all_gather(gate_weight, 'sp', axis=0, tiled=True)  81.3 us
    all_gather x1, waiting for transfers between devices, on_device(): value_piece = lax.all_gather(own_values, 'sp', axis=0, tiled=True)  44.8 us
    reduce_scatter x1, waiting for transfers between devices, on_device(): lax.psum_scatter(down_terms.astype(jnp.bfloat16), 'tp', scatter_dimension...  38 us
    reduce_scatter x1, waiting for transfers between devices, on_device(): lax.psum_scatter(projected, 'tp', scatter_dimension=1, tiled=True)  36.3 us
    all_gather x1, waiting for transfers between devices, on_device(): key_piece = lax.all_gather(key_matrix, 'sp', axis=0, tiled=True)  35.2 us
    all_gather x1, waiting for transfers between devices, on_device(): normed = lax.all_gather(normed_own, 'tp', axis=1, tiled=True)  30 us
  transfers between devices with their start and end apart: 8, of which 8 were waited for; matrix products, arithmetic and copies ran while one was open for 4% of the time, Pallas kernels for 0%

commit v1 on v0

v1 whole, which is shorter than its diff:
```python
import functools
import jax
import jax.numpy as jnp
from jax import lax
from jax.experimental import pallas as pl
from jax.experimental.pallas import tpu as pltpu
from jax.sharding import PartitionSpec as P

D = 2048
HEAD_SIZE = 128
QUERY_HEADS = 8
KEY_VALUE_HEADS = 2
GRID = 64

eps = 1e-06
rotary_base = 10000.0
MESH = pl.DeviceIdType.MESH
VMEM_LIMIT = 60 * 1024 * 1024
F32 = jnp.float32
BF16 = jnp.bfloat16


def apply_rotary(vectors, grid_positions):
    half_size = vectors.shape[-1] // 2
    frequency = rotary_base ** (-jnp.arange(0, half_size, 2, dtype=F32) / half_size)
    grid_row = (grid_positions // GRID).astype(F32)
    grid_col = (grid_positions % GRID).astype(F32)
    angles = jnp.concatenate(
        [grid_row[:, None] * frequency, grid_col[:, None] * frequency], axis=-1
    )[:, None, :]
    cosine_table = jnp.cos(angles)
    sine_table = jnp.sin(angles)
    first_half = vectors[..., :half_size]
    second_half = vectors[..., half_size:]
    return jnp.concatenate(
        [
            first_half * cosine_table - second_half * sine_table,
            first_half * sine_table + second_half * cosine_table,
        ],
        axis=-1,
    )


def per_head_norm(vectors, gain):
    return vectors * lax.rsqrt(jnp.mean(vectors * vectors, axis=-1, keepdims=True) + eps) * gain


def remote(src, dst, send, recv, sp, tp):
    copy = pltpu.make_async_remote_copy(
        src_ref=src, dst_ref=dst, send_sem=send, recv_sem=recv,
        device_id={"sp": sp, "tp": tp}, device_id_type=MESH,
    )
    copy.start()
    return copy


def greet(peers):
    barrier = pltpu.get_barrier_semaphore()
    for sp, tp in peers:
        pl.semaphore_signal(
            barrier, inc=1, device_id={"sp": sp, "tp": tp}, device_id_type=MESH
        )
    pl.semaphore_wait(barrier, len(peers))


def place():
    sp = lax.axis_index("sp")
    tp = lax.axis_index("tp")
    return sp, tp, sp // 2, lax.rem(sp, 2), tp // 2, lax.rem(tp, 2)


def gather_kernel(nz, kv_ref, out_ref, sz, rz, sy, ry, sc, rc):
    sp, tp, z, y, x, c = place()
    rows = kv_ref.shape[0]
    half = rows // 2
    other = x * 2 + (1 - c)
    z_peers = [lax.rem(z + k, nz) * 2 + y for k in range(1, nz)]
    y_peer = z * 2 + 1 - y
    greet([(p, tp) for p in z_peers] + [(y_peer, tp), (sp, other)])

    def spot(owner):
        return out_ref.at[pl.ds(pl.multiple_of(owner * rows + c * half, half), half), :]

    own = kv_ref.at[pl.ds(pl.multiple_of(c * half, half), half), :]
    sends = []
    to_z = [
        remote(own, spot(sp), sz.at[k - 1], rz.at[k - 1], z_peers[k - 1], tp)
        for k in range(1, nz)
    ]
    to_y = [remote(own, spot(sp), sy.at[0], ry.at[0], y_peer, tp)]
    out_ref[pl.ds(pl.multiple_of(sp * rows, rows), rows), :] = kv_ref[...]
    to_core = []
    for k in range(1, nz):
        to_z[k - 1].wait_recv()
        block = spot(lax.rem(z - k + nz, nz) * 2 + y)
        to_y.append(remote(block, block, sy.at[k], ry.at[k], y_peer, tp))
        to_core.append(remote(block, block, sc.at[k - 1], rc.at[k - 1], sp, other))
    for k in range(nz):
        to_y[k].wait_recv()
        block = spot(lax.rem(z - k + nz, nz) * 2 + 1 - y)
        slot = nz - 1 + k
        to_core.append(remote(block, block, sc.at[slot], rc.at[slot], sp, other))
    for copy in to_core:
        copy.wait_recv()
    for copy in to_z + to_y + to_core:
        copy.wait_send()


def gather_keys(kv, n_sp):
    nz = n_sp // 2
    dma = pltpu.SemaphoreType.DMA
    return pl.pallas_call(
        functools.partial(gather_kernel, nz),
        out_shape=jax.ShapeDtypeStruct((n_sp * kv.shape[0], kv.shape[1]), kv.dtype),
        in_specs=[pl.BlockSpec(memory_space=pltpu.VMEM)],
        out_specs=pl.BlockSpec(memory_space=pltpu.VMEM),
        scratch_shapes=[dma((nz - 1,)), dma((nz - 1,)), dma((nz,)), dma((nz,)),
                        dma((2 * nz - 1,)), dma((2 * nz - 1,))],
        compiler_params=pltpu.CompilerParams(collective_id=0, has_side_effects=True),
        name="gather_keys",
    )(kv)


def attend_kernel(width, q_ref, kv_ref, o_ref):
    rows = q_ref.shape[0]
    factor = HEAD_SIZE ** (-0.5) * 1.4426950408889634
    q = q_ref[...]

    def step(i, state):
        top, total, acc = state
        at = pl.ds(pl.multiple_of(i * width, width), width)
        s = lax.dot_general(
            q, kv_ref[at, 0:HEAD_SIZE], (((1,), (1,)), ((), ())), preferred_element_type=F32
        )
        new_top = jnp.maximum(top, jnp.max(s, axis=1, keepdims=True))
        fade = jnp.exp2((top - new_top) * factor)
        w = jnp.exp2((s - new_top) * factor)
        total = total * fade + jnp.sum(w, axis=1, keepdims=True)
        acc = acc * fade + jnp.dot(
            w.astype(BF16), kv_ref[at, HEAD_SIZE:], preferred_element_type=F32
        )
        return new_top, total, acc

    start = (
        jnp.full((rows, 1), -1e30, F32), jnp.zeros((rows, 1), F32),
        jnp.zeros((rows, HEAD_SIZE), F32),
    )
    top, total, acc = lax.fori_loop(0, kv_ref.shape[0] // width, step, start, unroll=2)
    o_ref[...] = (acc / total).astype(BF16)


def attend(queries, kv):
    rows, columns = queries.shape
    heads = columns // HEAD_SIZE
    block = 256
    width = 1024
    keys = kv.shape[0]
    work = rows * heads * keys
    return pl.pallas_call(
        functools.partial(attend_kernel, width),
        out_shape=jax.ShapeDtypeStruct((rows, columns), BF16),
        grid=(heads, rows // block),
        in_specs=[
            pl.BlockSpec((block, HEAD_SIZE), lambda h, i: (i, h)),
            pl.BlockSpec((keys, kv.shape[1]), lambda h, i: (0, 0)),
        ],
        out_specs=pl.BlockSpec((block, HEAD_SIZE), lambda h, i: (i, h)),
        compiler_params=pltpu.CompilerParams(vmem_limit_bytes=VMEM_LIMIT),
        cost_estimate=pl.CostEstimate(
            flops=work * HEAD_SIZE * 4, bytes_accessed=keys * 512, transcendentals=work
        ),
        name="attend",
    )(queries, kv)


def norm_kernel(nx, proj_ref, res_ref, gain_ref, mid_ref, out_ref,
                from_core, outgo, from_x, squares, blocks, s1, r1, s2, r2, s3, r3, s4, r4, s5, r5):
    sp, tp, z, y, x, c = place()
    rows, own = res_ref.shape
    n_tp = 2 * nx
    other = x * 2 + 1 - c
    y_peer = z * 2 + 1 - y
    xs = [lax.rem(x + j, nx) for j in range(nx)]
    back = [lax.rem(x - j + nx, nx) for j in range(nx)]
    row_peers = [(sp, xs[j] * 2 + c) for j in range(1, nx)]
    cross = [(y_peer, xs[j] * 2 + c) for j in range(nx)]
    across = [(sp, xs[j] * 2 + 1 - c) for j in range(1, nx)]
    greet([(sp, other)] + row_peers + cross + across)

    def cols(t):
        return pl.ds(pl.multiple_of(t * own, own), own)

    step = rows // 8
    to_core = [
        remote(proj_ref.at[:, cols(xs[j] * 2 + 1 - c)], from_core.at[j],
               s1.at[j], r1.at[j], sp, other)
        for j in list(range(1, nx)) + [0]
    ]
    to_core = [to_core[-1]] + to_core[:-1]
    to_x = []
    for j in range(1, nx):
        to_core[j].wait_recv()

        @pl.loop(0, 8)
        def _(i):
            at = pl.ds(pl.multiple_of(i * step, step), step)
            outgo[j - 1, at, :] = (
                proj_ref[at, cols(xs[j] * 2 + c)].astype(F32) + from_core[j, at, :].astype(F32)
            ).astype(BF16)

        to_x.append(remote(outgo.at[j - 1], from_x.at[j - 1], s2.at[j - 1], r2.at[j - 1],
                           *row_peers[j - 1]))
    to_core[0].wait_recv()
    for copy in to_x:
        copy.wait_recv()
    ones = jnp.ones((8, own), F32)

    for i in range(rows // 256):
        at = pl.ds(i * 256, 256)
        total = proj_ref[at, cols(tp)].astype(F32) + from_core[0, at, :].astype(F32)
        for j in range(1, nx):
            total += from_x[j - 1, at, :].astype(F32)
        mid = res_ref[at, :].astype(F32) + total
        mid_ref[at, :] = mid
        squares[0, :, at] = lax.dot_general(
            ones, mid * mid, (((1,), (1,)), ((), ())),
            precision=lax.Precision.HIGHEST, preferred_element_type=F32,
        )
    peers = [(sp, other)] + row_peers + across
    sq = [
        remote(squares.at[0], squares.at[k + 1], s3.at[k], r3.at[k], *peers[k])
        for k in range(len(peers))
    ]
    for copy in sq:
        copy.wait_recv()
    for i in range(rows // 256):
        at = pl.ds(i * 256, 256)
        square = squares[0, :, at]
        for k in range(len(peers)):
            square += squares[k + 1, :, at]
        scale = lax.rsqrt(square.T[:, 0:1] / (n_tp * own) + eps)
        blocks[at, :] = (mid_ref[at, :] * scale * gain_ref[...]).astype(BF16)

    def spot(yy, t):
        return out_ref.at[pl.ds(pl.multiple_of(yy * rows, rows), rows), cols(t)]

    targets = cross + row_peers
    sources = [(1 - y, back[j] * 2 + c) for j in range(nx)]
    sources += [(y, back[j] * 2 + c) for j in range(1, nx)]
    mine = spot(y, tp)
    far = [
        remote(blocks, mine, s4.at[k], r4.at[k], *targets[k]) for k in range(len(targets))
    ]
    near = [remote(blocks, mine, s5.at[0], r5.at[0], sp, other)]
    out_ref[pl.ds(pl.multiple_of(y * rows, rows), rows), cols(tp)] = blocks[...]
    for k in range(len(targets)):
        far[k].wait_recv()
        block = spot(*sources[k])
        near.append(remote(block, block, s5.at[k + 1], r5.at[k + 1], sp, other))
    for copy in near:
        copy.wait_recv()
    for copy in to_core + to_x + sq + far + near:
        copy.wait_send()


def project_norm(proj, res, gain, n_tp):
    nx = n_tp // 2
    rows, own = res.shape
    dma = pltpu.SemaphoreType.DMA
    n = 2 * nx
    vm = pl.BlockSpec(memory_space=pltpu.VMEM)
    return pl.pallas_call(
        functools.partial(norm_kernel, nx),
        out_shape=(
            jax.ShapeDtypeStruct((rows, own), F32),
            jax.ShapeDtypeStruct((2 * rows, n_tp * own), BF16),
        ),
        in_specs=[vm] * 3,
        out_specs=(vm, vm),
        scratch_shapes=[
            pltpu.VMEM((nx, rows, own), BF16),
            pltpu.VMEM((nx - 1, rows, own), BF16),
            pltpu.VMEM((nx - 1, rows, own), BF16),
            pltpu.VMEM((n, 8, rows), F32),
            pltpu.VMEM((rows, own), BF16),
            dma((nx,)), dma((nx,)), dma((nx - 1,)), dma((nx - 1,)),
            dma((n - 1,)), dma((n - 1,)), dma((n - 1,)), dma((n - 1,)), dma((n,)), dma((n,)),
        ],
        compiler_params=pltpu.CompilerParams(
            collective_id=1, has_side_effects=True, vmem_limit_bytes=VMEM_LIMIT
        ),
        name="project_norm",
    )(proj, res, gain)


def down_kernel(nx, terms_ref, mid_ref, out_ref, from_core, outgo, arrived, s1, r1, s2, r2):
    sp, tp, z, y, x, c = place()
    rows, own = mid_ref.shape
    other = x * 2 + 1 - c
    y_peer = z * 2 + 1 - y
    xs = [lax.rem(x + j, nx) for j in range(nx)]
    targets = [(y_peer, 1 - y, xs[j]) for j in range(nx)] + [(sp, y, xs[j]) for j in range(1, nx)]
    peers = [(s, xx * 2 + c) for s, yy, xx in targets]
    greet([(sp, other)] + peers)

    def spot(yy, t):
        return (pl.ds(pl.multiple_of(yy * rows, rows), rows),
                pl.ds(pl.multiple_of(t * own, own), own))

    every = targets + [(sp, y, x)]
    near = [
        remote(terms_ref.at[spot(yy, xx * 2 + 1 - c)], from_core.at[k], s1.at[k], r1.at[k],
               sp, other)
        for k, (s, yy, xx) in enumerate(every)
    ]
    step = rows // 8
    far = []
    for k, (s, yy, xx) in enumerate(targets):
        near[k].wait_recv()

        @pl.loop(0, 8)
        def _(i):
            at = pl.ds(pl.multiple_of(i * step, step), step)
            here = pl.ds(pl.multiple_of(yy * rows + i * step, step), step)
            outgo[k, at, :] = (
                terms_ref[here, spot(yy, xx * 2 + c)[1]].astype(F32)
                + from_core[k, at, :].astype(F32)
            ).astype(BF16)

        far.append(remote(outgo.at[k], arrived.at[k], s2.at[k], r2.at[k], *peers[k]))
    near[-1].wait_recv()
    for copy in far:
        copy.wait_recv()

    @pl.loop(0, 8)
    def _(i):
        at = pl.ds(pl.multiple_of(i * step, step), step)
        here = pl.ds(pl.multiple_of(y * rows + i * step, step), step)
        total = terms_ref[here, spot(y, tp)[1]].astype(F32)
        total += from_core[len(targets), at, :].astype(F32)
        for k in range(len(targets)):
            total += arrived[k, at, :].astype(F32)
        out_ref[at, :] = (mid_ref[at, :] + 0.5 * total).astype(BF16)

    for copy in near + far:
        copy.wait_send()


def down_sum(terms, mid, n_tp):
    nx = n_tp // 2
    rows, own = mid.shape
    dma = pltpu.SemaphoreType.DMA
    n = 2 * nx
    vm = pl.BlockSpec(memory_space=pltpu.VMEM)
    return pl.pallas_call(
        functools.partial(down_kernel, nx),
        out_shape=jax.ShapeDtypeStruct((rows, own), BF16),
        in_specs=[vm] * 2,
        out_specs=vm,
        scratch_shapes=[
            pltpu.VMEM((n, rows, own), BF16),
            pltpu.VMEM((n - 1, rows, own), BF16),
            pltpu.VMEM((n - 1, rows, own), BF16),
            dma((n,)), dma((n,)), dma((n - 1,)), dma((n - 1,)),
        ],
        compiler_params=pltpu.CompilerParams(
            collective_id=2, has_side_effects=True, vmem_limit_bytes=VMEM_LIMIT
        ),
        name="down_sum",
    )(terms, mid)


def on_device(n_sp, n_tp, residual_in, queries, keys, values, query_gain, key_norm_gain,
              out_weight, mlp_gain, gate_weight, up_weight, down_weight):
    local_rows = residual_in.shape[0]
    local_heads = queries.shape[1] // HEAD_SIZE
    queries_per_group = QUERY_HEADS // KEY_VALUE_HEADS
    tp_index = lax.axis_index("tp")
    sp_index = lax.axis_index("sp")
    low = lax.rem(sp_index, 2)

    pairs = [(i, i ^ 1) for i in range(n_sp)]
    lanes = [[i for i in range(n_sp) if i % 2 == r] for r in range(2)]
    units = gate_weight.shape[1] // 2

    def halves(weight, axis):
        keep = lax.dynamic_slice_in_dim(weight, low * units, units, axis)
        give = lax.dynamic_slice_in_dim(weight, (1 - low) * units, units, axis)
        return keep, give

    gate_keep, gate_give = halves(gate_weight, 1)
    up_keep, up_give = halves(up_weight, 1)
    down_keep, down_give = halves(down_weight, 0)
    both_keep = jnp.concatenate([gate_keep, up_keep], axis=1)
    both_got = lax.ppermute(jnp.concatenate([gate_give, up_give], axis=1), "sp", pairs)
    down_got = lax.ppermute(down_give, "sp", pairs)

    def ordered(kept, got, axis):
        return jnp.where(
            low == 0,
            jnp.concatenate([kept, got], axis=axis),
            jnp.concatenate([got, kept], axis=axis),
        )

    both = lax.all_gather(
        ordered(both_keep, both_got, 0), "sp", axis=0, axis_index_groups=lanes, tiled=True
    )
    down = lax.all_gather(
        ordered(down_keep, down_got, 1), "sp", axis=1, axis_index_groups=lanes, tiled=True
    )

    grid_positions = sp_index * local_rows + jnp.arange(local_rows, dtype=jnp.int32)
    shared = tp_index * local_heads // queries_per_group
    own_keys = lax.dynamic_slice_in_dim(keys, shared * HEAD_SIZE, HEAD_SIZE, 1)
    own_values = lax.dynamic_slice_in_dim(values, shared * HEAD_SIZE, HEAD_SIZE, 1)
    key_matrix = apply_rotary(
        per_head_norm(own_keys.astype(F32)[:, None, :], key_norm_gain), grid_positions
    )[:, 0, :].astype(BF16)
    kv = gather_keys(jnp.concatenate([key_matrix, own_values], axis=1), n_sp)
    query_rows = apply_rotary(
        per_head_norm(queries.astype(F32).reshape(local_rows, local_heads, HEAD_SIZE), query_gain),
        grid_positions,
    ).astype(BF16).reshape(local_rows, local_heads * HEAD_SIZE)
    attended = attend(query_rows, kv)
    projected = jnp.dot(attended, out_weight, preferred_element_type=F32).astype(BF16)
    own_width = residual_in.shape[1]
    gain_own = lax.dynamic_slice_in_dim(mlp_gain, tp_index * own_width, own_width, 0)[None, :]
    residual_mid, normed = project_norm(projected, residual_in, gain_own, n_tp)
    gate_up = jnp.dot(normed, both, preferred_element_type=F32)
    hidden = (jax.nn.silu(gate_up[:, :units]) * gate_up[:, units:]).astype(BF16)
    down_terms = jnp.dot(hidden, down, preferred_element_type=F32).astype(BF16)
    return down_sum(down_terms, residual_mid, n_tp)


def solution(mesh):
    in_specs = (
        P("sp", "tp"),
        P("sp", "tp"),
        P("sp", None),
        P("sp", None),
        P(),
        P(),
        P("tp", None),
        P(),
        P("sp", "tp"),
        P("sp", "tp"),
        P("tp", "sp"),
    )
    out_specs = P("sp", "tp")
    return jax.shard_map(
        functools.partial(on_device, mesh.shape["sp"], mesh.shape["tp"]),
        mesh=mesh, in_specs=in_specs, out_specs=out_specs, check_vma=False,
    )
```

time: 574 us -> 285 us (0.50)
  waiting for transfers between devices: 444 us -> 20.5 us
  Pallas kernels: 0 us -> 196 us
  matrix products: 62.2 us -> 29.2 us
  other arithmetic: 38.3 us -> 13.7 us
  blocking collectives: 5.99 us -> 0 us
    all_gather x6 -> x2, waiting for transfers between devices: 368 us -> 0.02 us  [the longest x1 0.02 us: on_device(): lax.all_gather(ordered(both_keep, both_got, 0), 'sp', axis=0, axis_index_...]
    pallas_call x0 -> x4, Pallas kernels: none -> 196 us  [the longest x1 73.2 us: project_norm(): pl.pallas_call(functools.partial(norm_kernel, nx), out_shape=(jax.ShapeDt...]
    reduce_scatter x2 -> x0, waiting for transfers between devices: 74.3 us -> none  [the longest x1 38 us: on_device(): lax.psum_scatter(down_terms.astype(jnp.bfloat16), 'tp', scatter_dimension...]
    dot_general x9 -> x3, matrix products: 62.2 us -> 29.2 us  [the longest x1 15.4 us: on_device(): gate_up = jnp.dot(normed, both, preferred_element_type=F32)]
    reduce_sum x4 -> x0, other arithmetic: 22 us -> none  [the longest x3 20.5 us: one_block(): running_sum = running_sum * factor + jnp.sum(weights, axis=1)]
    ppermute x0 -> x2, waiting for transfers between devices: none -> 20.4 us  [the longest x1 16.2 us: on_device(): lax.ppermute(jnp.concatenate([gate_give, up_give], axis=1), 'sp', pairs)]
    psum x1 -> x0, blocking collectives: 5.99 us -> none  [on_device(): squares = lax.psum(jnp.sum(residual_mid * residual_mid, axis=1), 'tp')]
  transfers between devices with their start and end apart: 8 -> 4, of which waited for: 8 -> 2; matrix products, arithmetic and copies ran while one was open for 4% -> 12% of each run, Pallas kernels for 0% -> 53%
where the time goes in v1:
time: 285 us
  Pallas kernels  196 us (69%)
  matrix products  29.2 us (10%)
  waiting for transfers between devices  20.5 us (7%)
  other arithmetic  13.7 us (5%)
  between operations  13.6 us (5%)
  local copies, waits for them, and re-layouts  7.88 us (3%)
  starting transfers between devices  3.21 us (1%)
    pallas_call x1, Pallas kernels, project_norm(): pl.pallas_call(functools.partial(norm_kernel, nx), out_shape=(jax.ShapeDt...  73.2 us
    pallas_call x1, Pallas kernels, gather_keys(): pl.pallas_call(functools.partial(gather_kernel, nz), out_shape=jax.ShapeD...  54.6 us
    pallas_call x1, Pallas kernels, down_sum(): pl.pallas_call(functools.partial(down_kernel, nx), out_shape=jax.ShapeDty...  45.2 us
    pallas_call x1, Pallas kernels, attend(): pl.pallas_call(functools.partial(attend_kernel, width), out_shape=jax.Sha...  23.5 us
    ppermute x1, waiting for transfers between devices, on_device(): lax.ppermute(jnp.concatenate([gate_give, up_give], axis=1), 'sp', pairs)  16.2 us
    dot_general x1, matrix products, on_device(): gate_up = jnp.dot(normed, both, preferred_element_type=F32)  15.4 us
    dot_general x1, matrix products, on_device(): down_terms = jnp.dot(hidden, down, preferred_element_type=F32).astype(BF16)  10.2 us
  transfers between devices with their start and end apart: 4, of which 2 were waited for; matrix products, arithmetic and copies ran while one was open for 12% of the time, Pallas kernels for 53%

profile of v1, /device:TPU:24, one launch (start us, length us, event | category | flops | bytes accessed | tf_op | source)
XLA Modules:
  0.0 284.7 jit_solution(3607691023964791981)
XLA Ops:
  6.5 2.2 constant_dynamic-slice_fusion.4
  8.8 0.2 pad_maximum_fusion.1
  9.0 1.6 collective-permute-start
  10.6 0.2 pad_maximum_fusion
  10.8 16.2 %collective-permute-done = bf16[256,1408]{1,0:T(8,128)(2,1)} collective-permute-done((bf16[256,1408]{1,0:T(8,128)(2,1)S(1)}, bf16[256,1408]{1,0:T(8,128)(2,1)}, u32[]{:S(2)}, u32[]{:S(2)}) %collective-permute-start) | collective-permute-done | bytes 720928 | tf_op jit(solution)/shard_map/ppermute | solution.py:395
  27.0 2.8 maximum_select_fusion
  30.0 1.6 collective-permute-start.1
  31.6 0.2 fusion.3
  31.8 0.9 constant_dynamic-slice_fusion.6
  32.8 0.2 fusion.5
  33.0 0.3 fusion.10
  33.2 1.8 subtract_convert_fusion.1
  35.0 0.1 maximum_bitcast_fusion
  35.2 4.2 %collective-permute-done.1 = bf16[704,256]{1,0:T(8,128)(2,1)S(1)} collective-permute-done((bf16[704,256]{1,0:T(8,128)(2,1)S(1)}, bf16[704,256]{1,0:T(8,128)(2,1)S(1)}, u32[]{:S(2)}, u32[]{:S(2)}) %collective-permute-start.1) | collective-permute-done | bytes 360480 | tf_op jit(solution)/shard_map/ppermute | solution.py:396
  39.4 1.0 maximum_select_fusion.1
  40.4 0.8 pad_maximum_fusion.5.kv_ref
  41.2 54.6 %gather_keys.1.kv_ref = bf16[6144,256]{1,0:T(8,128)(2,1)} custom-call(bf16[768,256]{1,0:T(8,128)(2,1)} %pad_maximum_fusion.5.kv_ref), custom_call_target="tpu_custom_call" | custom-call | tf_op jit(solution)/shard_map/gather_keys/pallas_call | solution.py:112
  95.9 0.4 reshape.222
  96.3 1.7 fusion.9
  97.9 0.9 multiply_reduce_fusion
  98.9 1.0 multiply_multiply_fusion
  99.9 1.4 subtract_convert_fusion
  101.3 1.1 pad_maximum_fusion.3
  102.4 0.8 copy.18
  103.2 1.4 dynamic_slice.29
  104.6 23.5 %attend.1 = bf16[768,256]{1,0:T(8,128)(2,1)} custom-call(bf16[768,256]{1,0:T(8,128)(2,1)} %bitcast.19, bf16[6144,256]{1,0:T(8,128)(2,1)} %gather_keys.1.kv_ref), custom_call_target="tpu_custom_call" | custom-call | flops 4831838208 | bytes 3145728 | tf_op jit(solution)/shard_map/attend/pallas_call | solution.py:159
  128.1 3.6 %convolution_convert_fusion.1.proj_ref = bf16[768,2048]{1,0:T(8,128)(2,1)} fusion(bf16[768,256]{1,0:T(8,128)(2,1)} %attend.1, bf16[256,2048]{1,0:T(8,128)(2,1)S(1)} %copy-done), kind=kOutput, calls=%fused_computation.3 | convolution fusion | flops 806879232 | bytes 4587520 | tf_op jit(solution)/shard_map/dot_general | solution.py:425
  131.7 73.2 %project_norm.1 = (f32[768,512]{1,0:T(8,128)}, bf16[1536,2048]{1,0:T(8,128)(2,1)}) custom-call(bf16[768,2048]{1,0:T(8,128)(2,1)} %convolution_convert_fusion.1.proj_ref, bf16[768,512]{1,0:T(8,128)(2,1)} %res_ref.1, f32[1,512]{1,0:T(1,128)} %bitcast.20), custom_call_target="tpu_custom_call" | custom-call | tf_op jit(solution)/shard_map/project_norm/pallas_call | solution.py:272
  204.9 15.4 %fusion.20 = f32[1536,1408]{0,1:T(8,128)} fusion(bf16[1536,2048]{1,0:T(8,128)(2,1)} %get-tuple-element.7, bf16[2048,1408]{1,0:T(8,128)(2,1)} %all-gather.3.cloned.1.call-done), kind=kOutput, calls=%fused_computation.59 | convolution fusion | flops 8858370048 | bytes 20709376 | tf_op jit(solution)/shard_map/dot_general | solution.py:429
  220.3 10.2 %convolution_convert_fusion.terms_ref = bf16[1536,2048]{1,0:T(8,128)(2,1)} fusion(bf16[704,2048]{1,0:T(8,128)(2,1)} %all-gather.5.cloned.1.call-done, f32[1536,1408]{0,1:T(8,128)} %fusion.20), kind=kOutput, calls=%fused_computation | convolution fusion | flops 4438818816 | bytes 17825792 | tf_op jit(solution)/shard_map/dot_general | solution.py:431
  230.6 45.2 %down_sum.1 = bf16[768,512]{1,0:T(8,128)(2,1)} custom-call(bf16[1536,2048]{1,0:T(8,128)(2,1)} %convolution_convert_fusion.terms_ref, f32[768,512]{1,0:T(8,128)} %get-tuple-element.8.mid_ref), custom_call_target="tpu_custom_call" | custom-call | tf_op jit(solution)/shard_map/down_sum/pallas_call | solution.py:355
  275.8 2.1 copy.20
  (23 shorter events, 0.3 us)
Async XLA Ops:
  6.5 121.5 %copy-start = (bf16[256,2048]{1,0:T(8,128)(2,1)S(1)}, bf16[256,2048]{1,0:T(8,128)(2,1)}, u32[]{:S(2)}) copy-start(bf16[256,2048]{1,0:T(8,128)(2,1)} %param.17) | copy-start | bytes 3145732
  6.5 198.4 %all-gather.3.cloned.1.call-start = ((), (), s32[]{:S(2)}) async-start(), calls=%async_computation | async-start | bytes 7208960 | tf_op jit(solution)/shard_map/all_gather | solution.py:405
  9.0 18.0 %collective-permute-start = (bf16[256,1408]{1,0:T(8,128)(2,1)S(1)}, bf16[256,1408]{1,0:T(8,128)(2,1)}, u32[]{:S(2)}, u32[]{:S(2)}) collective-permute-start(bf16[256,1408]{1,0:T(8,128)(2,1)S(1)} %pad_maximum_fusion.1), channel_id=1, source_target_pairs={{0,4},{4,0},{8,12},{12,8},{16,20},{20,16},{24,28},{28,24},{1,5},{5... | collective-permute-start | bytes 2162696 | tf_op jit(solution)/shard_map/ppermute | solution.py:395
  10.6 19.4 %copy-start.1 = (bf16[1408,256]{1,0:T(8,128)(2,1)S(1)}, bf16[1408,256]{1,0:T(8,128)(2,1)}, u32[]{:S(2)}) copy-start(bf16[1408,256]{1,0:T(8,128)(2,1)} %param.21) | copy-start | bytes 2162692
  10.8 20.8 %copy-start.2 = (bf16[768,256]{1,0:T(8,128)(2,1)S(1)}, bf16[768,256]{1,0:T(8,128)(2,1)}, u32[]{:S(2)}) copy-start(bf16[768,256]{1,0:T(8,128)(2,1)} %param.13) | copy-start | bytes 1179652
  10.8 22.0 %copy-start.4 = (f32[128]{0:T(128)S(1)}, f32[128]{0:T(128)}, u32[]{:S(2)}) copy-start(f32[128]{0:T(128)} %param.16) | copy-start | bytes 1540
  29.9 190.4 %all-gather.5.cloned.1.call-start = ((), (), s32[]{:S(2)}) async-start(), calls=%async_computation.1 | async-start | bytes 3604480 | tf_op jit(solution)/shard_map/all_gather | solution.py:408
  30.0 9.4 %collective-permute-start.1 = (bf16[704,256]{1,0:T(8,128)(2,1)S(1)}, bf16[704,256]{1,0:T(8,128)(2,1)S(1)}, u32[]{:S(2)}, u32[]{:S(2)}) collective-permute-start(bf16[704,256]{1,0:T(8,128)(2,1)S(1)} %get-tuple-element.20), channel_id=1, source_target_pairs={{0,4},{4,0},{8,12},{12,8},{16,20},{20,16},{24,28},{28,24},{1,5},{5... | collective-permute-start | bytes 1081352 | tf_op jit(solution)/shard_map/ppermute | solution.py:396
  40.4 55.5 %copy-start.3 = (bf16[768,256]{1,0:T(8,128)(2,1)S(1)}, bf16[768,256]{1,0:T(8,128)(2,1)}, u32[]{:S(2)}) copy-start(bf16[768,256]{1,0:T(8,128)(2,1)} %param.12) | copy-start | bytes 1179652
  95.9 3.0 %copy-start.5 = (f32[128]{0:T(128)S(1)}, f32[128]{0:T(128)}, u32[]{:S(2)}) copy-start(f32[128]{0:T(128)} %param.15) | copy-start | bytes 1540
Sparse Core Ops, SparseCore 0:
  30.0 121.3 all-gather.2
  153.0 57.6 all-gather.4

commit v2 on v1

--- a/solution.py
+++ b/solution.py
@@ -239,24 +239,38 @@
         for k in range(len(peers)):
             square += squares[k + 1, :, at]
         scale = lax.rsqrt(square.T[:, 0:1] / (n_tp * own) + eps)
-        blocks[at, :] = (mid_ref[at, :] * scale * gain_ref[...]).astype(BF16)
+        block = (mid_ref[at, :] * scale * gain_ref[...]).astype(BF16)
+        blocks[0, at, :] = block[:, : own // 2]
+        blocks[1, at, :] = block[:, own // 2 :]
+
+    half = own // 2
 
     def spot(yy, t):
-        return out_ref.at[pl.ds(pl.multiple_of(yy * rows, rows), rows), cols(t)]
+        return (pl.ds(pl.multiple_of(yy * rows, rows), rows),
+                pl.ds(pl.multiple_of(t * half, half), half))
 
     targets = cross + row_peers
     sources = [(1 - y, back[j] * 2 + c) for j in range(nx)]
     sources += [(y, back[j] * 2 + c) for j in range(1, nx)]
     mine = spot(y, tp)
-    far = [
-        remote(blocks, mine, s4.at[k], r4.at[k], *targets[k]) for k in range(len(targets))
-    ]
-    near = [remote(blocks, mine, s5.at[0], r5.at[0], sp, other)]
-    out_ref[pl.ds(pl.multiple_of(y * rows, rows), rows), cols(tp)] = blocks[...]
+    far = []
     for k in range(len(targets)):
-        far[k].wait_recv()
-        block = spot(*sources[k])
-        near.append(remote(block, block, s5.at[k + 1], r5.at[k + 1], sp, other))
+        side = 1 - y if k < nx else y
+        for i in range(2):
+            at = (lax.rem(i + side, 2),) + mine
+            far.append(remote(blocks.at[i], out_ref.at[at], s4.at[2 * k + i], r4.at[2 * k + i],
+                              *targets[k]))
+    near = []
+    for i in range(2):
+        at = (lax.rem(i + y, 2),) + mine
+        near.append(remote(blocks.at[i], out_ref.at[at], s5.at[i], r5.at[i], sp, other))
+        out_ref[at] = blocks[i]
+    for k in range(len(targets)):
+        for i in range(2):
+            far[2 * k + i].wait_recv()
+            at = (lax.rem(i + y, 2),) + spot(*sources[k])
+            slot = 2 * k + 2 + i
+            near.append(remote(out_ref.at[at], out_ref.at[at], s5.at[slot], r5.at[slot], sp, other))
     for copy in near:
         copy.wait_recv()
     for copy in to_core + to_x + sq + far + near:
@@ -273,7 +287,7 @@
         functools.partial(norm_kernel, nx),
         out_shape=(
             jax.ShapeDtypeStruct((rows, own), F32),
-            jax.ShapeDtypeStruct((2 * rows, n_tp * own), BF16),
+            jax.ShapeDtypeStruct((2, 2 * rows, n_tp * own // 2), BF16),
         ),
         in_specs=[vm] * 3,
         out_specs=(vm, vm),
@@ -282,9 +296,10 @@
             pltpu.VMEM((nx - 1, rows, own), BF16),
             pltpu.VMEM((nx - 1, rows, own), BF16),
             pltpu.VMEM((n, 8, rows), F32),
-            pltpu.VMEM((rows, own), BF16),
+            pltpu.VMEM((2, rows, own // 2), BF16),
             dma((nx,)), dma((nx,)), dma((nx - 1,)), dma((nx - 1,)),
-            dma((n - 1,)), dma((n - 1,)), dma((n - 1,)), dma((n - 1,)), dma((n,)), dma((n,)),
+            dma((n - 1,)), dma((n - 1,)), dma((2 * n - 2,)), dma((2 * n - 2,)),
+            dma((2 * n,)), dma((2 * n,)),
         ],
         compiler_params=pltpu.CompilerParams(
             collective_id=1, has_side_effects=True, vmem_limit_bytes=VMEM_LIMIT
@@ -293,29 +308,33 @@
     )(proj, res, gain)
 
 
-def down_kernel(nx, terms_ref, mid_ref, out_ref, from_core, outgo, arrived, s1, r1, s2, r2):
+def down_kernel(nx, terms_ref, mid_ref, out_ref, from_core, outgo, from_y, from_x, relay,
+                last_x, last_y, s1, r1, s2, r2, s3, r3, s4, r4, s5, r5):
     sp, tp, z, y, x, c = place()
     rows, own = mid_ref.shape
+    half = rows // 2
+    top, low = pl.ds(0, half), pl.ds(half, half)
     other = x * 2 + 1 - c
-    y_peer = z * 2 + 1 - y
+    y_peer = (z * 2 + 1 - y, tp)
     xs = [lax.rem(x + j, nx) for j in range(nx)]
-    targets = [(y_peer, 1 - y, xs[j]) for j in range(nx)] + [(sp, y, xs[j]) for j in range(1, nx)]
-    peers = [(s, xx * 2 + c) for s, yy, xx in targets]
-    greet([(sp, other)] + peers)
-
-    def spot(yy, t):
-        return (pl.ds(pl.multiple_of(yy * rows, rows), rows),
-                pl.ds(pl.multiple_of(t * own, own), own))
-
-    every = targets + [(sp, y, x)]
-    near = [
-        remote(terms_ref.at[spot(yy, xx * 2 + 1 - c)], from_core.at[k], s1.at[k], r1.at[k],
-               sp, other)
-        for k, (s, yy, xx) in enumerate(every)
-    ]
+    x_peers = [(sp, xs[j] * 2 + c) for j in range(nx)]
+    greet([(sp, other), y_peer] + x_peers[1:])
+    every = [(1 - y, xs[j]) for j in range(nx)] + [(y, xs[j]) for j in range(1, nx)] + [(y, x)]
+    order = list(range(1, 2 * nx - 1)) + [0, 2 * nx - 1]
+
+    def cols(t):
+        return pl.ds(pl.multiple_of(t * own, own), own)
+
+    near = {}
+    for k in order:
+        yy, xx = every[k]
+        near[k] = remote(
+            terms_ref.at[pl.ds(pl.multiple_of(yy * rows, rows), rows), cols(xx * 2 + 1 - c)],
+            from_core.at[k], s1.at[k], r1.at[k], sp, other)
     step = rows // 8
-    far = []
-    for k, (s, yy, xx) in enumerate(targets):
+    to_y, to_x, again = {}, {}, []
+    for k in order[:-1]:
+        yy, xx = every[k]
         near[k].wait_recv()
 
         @pl.loop(0, 8)
@@ -323,26 +342,63 @@
             at = pl.ds(pl.multiple_of(i * step, step), step)
             here = pl.ds(pl.multiple_of(yy * rows + i * step, step), step)
             outgo[k, at, :] = (
-                terms_ref[here, spot(yy, xx * 2 + c)[1]].astype(F32)
-                + from_core[k, at, :].astype(F32)
+                terms_ref[here, cols(xx * 2 + c)].astype(F32) + from_core[k, at, :].astype(F32)
             ).astype(BF16)
 
-        far.append(remote(outgo.at[k], arrived.at[k], s2.at[k], r2.at[k], *peers[k]))
-    near[-1].wait_recv()
-    for copy in far:
-        copy.wait_recv()
-
-    @pl.loop(0, 8)
+        if k < nx:
+            to_y[k] = remote(outgo.at[k, top], from_y.at[k], s2.at[k], r2.at[k], *y_peer)
+        j = k if k < nx else k - nx + 1
+        if j > 0:
+            slot = 2 * (j - 1) + (1 if k < nx else 0)
+            to_x[slot] = remote(outgo.at[k, low], from_x.at[slot], s3.at[slot], r3.at[slot],
+                                *x_peers[j])
+    for j in range(1, nx):
+        to_y[j].wait_recv()
+
+        @pl.loop(0, 4)
+        def _(i):
+            at = pl.ds(pl.multiple_of(i * step, step), step)
+            relay[j, at, :] = (
+                outgo[nx + j - 1, at, :].astype(F32) + from_y[j, at, :].astype(F32)
+            ).astype(BF16)
+
+        again.append(remote(relay.at[j], last_x.at[j - 1], s4.at[j - 1], r4.at[j - 1],
+                            *x_peers[j]))
+    for j in range(1, nx):
+        to_x[2 * j - 1].wait_recv()
+
+    @pl.loop(0, 4)
     def _(i):
         at = pl.ds(pl.multiple_of(i * step, step), step)
-        here = pl.ds(pl.multiple_of(y * rows + i * step, step), step)
-        total = terms_ref[here, spot(y, tp)[1]].astype(F32)
-        total += from_core[len(targets), at, :].astype(F32)
-        for k in range(len(targets)):
-            total += arrived[k, at, :].astype(F32)
-        out_ref[at, :] = (mid_ref[at, :] + 0.5 * total).astype(BF16)
-
-    for copy in near + far:
+        here = pl.ds(pl.multiple_of(half + i * step, step), step)
+        total = outgo[0, here, :].astype(F32)
+        for j in range(1, nx):
+            total += from_x[2 * j - 1, at, :].astype(F32)
+        relay[0, at, :] = total.astype(BF16)
+
+    again.append(remote(relay.at[0], last_y, s5.at[0], r5.at[0], *y_peer))
+    near[2 * nx - 1].wait_recv()
+    to_y[0].wait_recv()
+    for j in range(1, nx):
+        to_x[2 * j - 2].wait_recv()
+    for copy in again:
+        copy.wait_recv()
+
+    @pl.loop(0, 4)
+    def _(i):
+        at = pl.ds(pl.multiple_of(i * step, step), step)
+        for part in range(2):
+            to = pl.ds(pl.multiple_of(part * half + i * step, step), step)
+            here = pl.ds(pl.multiple_of(y * rows + part * half + i * step, step), step)
+            total = terms_ref[here, cols(tp)].astype(F32)
+            total += from_core[2 * nx - 1, to, :].astype(F32)
+            total += (from_y[0, at, :] if part == 0 else last_y[at, :]).astype(F32)
+            for j in range(1, nx):
+                total += (last_x[j - 1, at, :] if part == 0
+                          else from_x[2 * j - 2, at, :]).astype(F32)
+            out_ref[to, :] = (mid_ref[to, :] + 0.5 * total).astype(BF16)
+
+    for copy in list(near.values()) + list(to_y.values()) + list(to_x.values()) + again:
         copy.wait_send()
 
 
@@ -360,8 +416,13 @@
         scratch_shapes=[
             pltpu.VMEM((n, rows, own), BF16),
             pltpu.VMEM((n - 1, rows, own), BF16),
-            pltpu.VMEM((n - 1, rows, own), BF16),
-            dma((n,)), dma((n,)), dma((n - 1,)), dma((n - 1,)),
+            pltpu.VMEM((nx, rows // 2, own), BF16),
+            pltpu.VMEM((n - 2, rows // 2, own), BF16),
+            pltpu.VMEM((nx, rows // 2, own), BF16),
+            pltpu.VMEM((nx - 1, rows // 2, own), BF16),
+            pltpu.VMEM((rows // 2, own), BF16),
+            dma((n,)), dma((n,)), dma((nx,)), dma((nx,)), dma((n - 2,)), dma((n - 2,)),
+            dma((nx - 1,)), dma((nx - 1,)), dma((1,)), dma((1,)),
         ],
         compiler_params=pltpu.CompilerParams(
             collective_id=2, has_side_effects=True, vmem_limit_bytes=VMEM_LIMIT
@@ -402,13 +463,9 @@
             jnp.concatenate([got, kept], axis=axis),
         )
 
-    both = lax.all_gather(
-        ordered(both_keep, both_got, 0), "sp", axis=0, axis_index_groups=lanes, tiled=True
-    )
-    down = lax.all_gather(
-        ordered(down_keep, down_got, 1), "sp", axis=1, axis_index_groups=lanes, tiled=True
-    )
-
+    both_first = lax.all_gather(
+        both_keep, "sp", axis=0, axis_index_groups=lanes, tiled=True
+    )
     grid_positions = sp_index * local_rows + jnp.arange(local_rows, dtype=jnp.int32)
     shared = tp_index * local_heads // queries_per_group
     own_keys = lax.dynamic_slice_in_dim(keys, shared * HEAD_SIZE, HEAD_SIZE, 1)
@@ -416,17 +473,28 @@
     key_matrix = apply_rotary(
         per_head_norm(own_keys.astype(F32)[:, None, :], key_norm_gain), grid_positions
     )[:, 0, :].astype(BF16)
-    kv = gather_keys(jnp.concatenate([key_matrix, own_values], axis=1), n_sp)
     query_rows = apply_rotary(
         per_head_norm(queries.astype(F32).reshape(local_rows, local_heads, HEAD_SIZE), query_gain),
         grid_positions,
     ).astype(BF16).reshape(local_rows, local_heads * HEAD_SIZE)
+    own_kv, query_rows, both_got, down_got = lax.optimization_barrier(
+        (jnp.concatenate([key_matrix, own_values], axis=1), query_rows, both_got, down_got)
+    )
+    both_second = lax.all_gather(
+        both_got, "sp", axis=0, axis_index_groups=lanes, tiled=True
+    )
+    down = lax.all_gather(
+        ordered(down_keep, down_got, 1), "sp", axis=1, axis_index_groups=lanes, tiled=True
+    )
+    kv = gather_keys(own_kv, n_sp)
     attended = attend(query_rows, kv)
     projected = jnp.dot(attended, out_weight, preferred_element_type=F32).astype(BF16)
     own_width = residual_in.shape[1]
     gain_own = lax.dynamic_slice_in_dim(mlp_gain, tp_index * own_width, own_width, 0)[None, :]
     residual_mid, normed = project_norm(projected, residual_in, gain_own, n_tp)
-    gate_up = jnp.dot(normed, both, preferred_element_type=F32)
+    assert n_sp == 2 * n_tp
+    gate_up = jnp.dot(normed[0], both_first, preferred_element_type=F32)
+    gate_up += jnp.dot(normed[1], both_second, preferred_element_type=F32)
     hidden = (jax.nn.silu(gate_up[:, :units]) * gate_up[:, units:]).astype(BF16)
     down_terms = jnp.dot(hidden, down, preferred_element_type=F32).astype(BF16)
     return down_sum(down_terms, residual_mid, n_tp)

time: 285 us -> 274 us (0.961)
  Pallas kernels: 196 us -> 185 us
  waiting for transfers between devices: 20.5 us -> 11.4 us
  matrix products: 29.2 us -> 38 us
    ppermute x1, waiting for transfers between devices: 16.2 us -> 0.01 us  [on_device(): lax.ppermute(jnp.concatenate([gate_give, up_give], axis=1), 'sp', pairs)]
    pallas_call x1, Pallas kernels: 45.2 us -> 35.5 us  [down_sum(): pl.pallas_call(functools.partial(down_kernel, nx), out_shape=jax.ShapeDty...]
    dot_general x1 -> x2, matrix products: 15.4 us -> 24.1 us  [the longest x1 13.3 us: on_device(): gate_up += jnp.dot(normed[1], both_second, preferred_element_type=F32)]
    ppermute x1, waiting for transfers between devices: 4.2 us -> 11.3 us  [on_device(): down_got = lax.ppermute(down_give, 'sp', pairs)]
  transfers between devices with their start and end apart: 4 -> 5, of which waited for: 2 -> 1; matrix products, arithmetic and copies ran while one was open for 12% -> 16% of each run, Pallas kernels for 53% -> 55%
where the time goes in v2:
time: 274 us
  Pallas kernels  185 us (68%)
  matrix products  38 us (14%)
  other arithmetic  13.7 us (5%)
  between operations  13.3 us (5%)
  waiting for transfers between devices  11.4 us (4%)
  local copies, waits for them, and re-layouts  9.61 us (4%)
    pallas_call x1, Pallas kernels, project_norm(): pl.pallas_call(functools.partial(norm_kernel, nx), out_shape=(jax.ShapeDt...  72.9 us
    pallas_call x1, Pallas kernels, gather_keys(): pl.pallas_call(functools.partial(gather_kernel, nz), out_shape=jax.ShapeD...  53.3 us
    pallas_call x1, Pallas kernels, down_sum(): pl.pallas_call(functools.partial(down_kernel, nx), out_shape=jax.ShapeDty...  35.5 us
    pallas_call x1, Pallas kernels, attend(): pl.pallas_call(functools.partial(attend_kernel, width), out_shape=jax.Sha...  23.6 us
    dot_general x1, matrix products, on_device(): gate_up += jnp.dot(normed[1], both_second, preferred_element_type=F32)  13.3 us
    ppermute x1, waiting for transfers between devices, on_device(): down_got = lax.ppermute(down_give, 'sp', pairs)  11.3 us
    dot_general x1, matrix products, on_device(): gate_up = jnp.dot(normed[0], both_first, preferred_element_type=F32)  10.8 us
    dot_general x1, matrix products, on_device(): down_terms = jnp.dot(hidden, down, preferred_element_type=F32).astype(BF16)  10.2 us
  transfers between devices with their start and end apart: 5, of which 1 were waited for; matrix products, arithmetic and copies ran while one was open for 16% of the time, Pallas kernels for 55%

profile of v2, /device:TPU:24, one launch (start us, length us, event | category | flops | bytes accessed | tf_op | source)
XLA Modules:
  0.0 273.6 jit_solution(17227365561765870275)
XLA Ops:
  6.5 2.2 constant_dynamic-slice_fusion.1
  8.8 1.1 pad_maximum_fusion.1
  10.0 1.1 pad_maximum_fusion
  11.0 1.5 collective-permute-start
  12.6 0.8 constant_dynamic-slice_fusion
  13.3 0.5 collective-permute-start.1
  13.9 1.4 reshape.222
  15.3 0.2 fusion.8
  15.5 0.3 broadcast_multiply_fusion.1
  15.8 1.7 fusion.12
  17.4 0.9 multiply_reduce_fusion
  18.4 0.2 fusion.10
  18.6 1.0 multiply_multiply_fusion
  19.6 1.4 subtract_convert_fusion
  21.0 1.8 subtract_convert_fusion.1
  22.8 1.1 pad_maximum_fusion.5
  23.9 0.8 copy.18
  24.7 0.1 maximum_bitcast_fusion
  24.8 0.8 pad_maximum_fusion.3.kv_ref
  25.6 11.3 %collective-permute-done.1 = bf16[704,256]{1,0:T(8,128)(2,1)} collective-permute-done((bf16[704,256]{1,0:T(8,128)(2,1)}, bf16[704,256]{1,0:T(8,128)(2,1)}, u32[]{:S(2)}, u32[]{:S(2)}) %collective-permute-start.1) | collective-permute-done | bytes 360480 | tf_op jit(solution)/shard_map/ppermute | solution.py:457
  37.0 0.9 copy-done.2
  38.0 2.1 maximum_select_fusion
  40.1 1.3 dynamic_slice.32
  41.5 53.3 %gather_keys.1.kv_ref = bf16[6144,256]{1,0:T(8,128)(2,1)} custom-call(bf16[768,256]{1,0:T(8,128)(2,1)} %pad_maximum_fusion.3.kv_ref), custom_call_target="tpu_custom_call" | custom-call | tf_op jit(solution)/shard_map/gather_keys/pallas_call | solution.py:112
  94.8 23.6 %attend.1 = bf16[768,256]{1,0:T(8,128)(2,1)} custom-call(bf16[768,256]{1,0:T(8,128)(2,1)} %bitcast.25, bf16[6144,256]{1,0:T(8,128)(2,1)} %gather_keys.1.kv_ref), custom_call_target="tpu_custom_call" | custom-call | flops 4831838208 | bytes 3145728 | tf_op jit(solution)/shard_map/attend/pallas_call | solution.py:159
  118.5 3.6 %convolution_convert_fusion.1.proj_ref = bf16[768,2048]{1,0:T(8,128)(2,1)} fusion(bf16[768,256]{1,0:T(8,128)(2,1)} %attend.1, bf16[256,2048]{1,0:T(8,128)(2,1)S(1)} %copy-done), kind=kOutput, calls=%fused_computation.4 | convolution fusion | flops 806879232 | bytes 4587520 | tf_op jit(solution)/shard_map/dot_general | solution.py:491
  122.1 72.9 %project_norm.1 = (f32[768,512]{1,0:T(8,128)}, bf16[2,1536,1024]{2,1,0:T(8,128)(2,1)}) custom-call(bf16[768,2048]{1,0:T(8,128)(2,1)} %convolution_convert_fusion.1.proj_ref, bf16[768,512]{1,0:T(8,128)(2,1)} %res_ref.1, f32[1,512]{1,0:T(1,128)} %bitcast.26), custom_call_target="tpu_custom_call" | custom-call | tf_op jit(solution)/shard_map/project_norm/pallas_call | solution.py:286
  195.1 10.8 %fusion.2 = f32[1536,1408]{0,1:T(8,128)} fusion(bf16[1024,1408]{1,0:T(8,128)(2,1)} %all-gather.4.cloned.1.call-done, bf16[2,1536,1024]{2,1,0:T(8,128)(2,1)} %get-tuple-element.13), kind=kOutput, calls=%fused_computation.6 | convolution fusion | flops 4429185024 | bytes 14680064 | tf_op jit(solution)/shard_map/dot_general | solution.py:496
  205.9 13.3 %convolution_add_fusion = f32[1536,1408]{0,1:T(8,128)} fusion(f32[1536,1408]{0,1:T(8,128)} %fusion.2, bf16[1024,1408]{1,0:T(8,128)(2,1)} %all-gather.6.cloned.1.call-done, bf16[2,1536,1024]{2,1,0:T(8,128)(2,1)} %get-tuple-element.13), kind=kOutput, calls=%fused_computation | convolution fusion | flops 4431347712 | bytes 23330816 | tf_op jit(solution)/shard_map/dot_general | solution.py:497
  219.2 10.2 %convolution_convert_fusion.terms_ref = bf16[1536,2048]{1,0:T(8,128)(2,1)} fusion(bf16[704,2048]{1,0:T(8,128)(2,1)} %all-gather.8.cloned.1.call-done, f32[1536,1408]{0,1:T(8,128)} %convolution_add_fusion), kind=kOutput, calls=%fused_computation.1 | convolution fusion | flops 4438818816 | bytes 17825792 | tf_op jit(solution)/shard_map/dot_general | solution.py:499
  229.4 35.5 %down_sum.1 = bf16[768,512]{1,0:T(8,128)(2,1)} custom-call(bf16[1536,2048]{1,0:T(8,128)(2,1)} %convolution_convert_fusion.terms_ref, f32[768,512]{1,0:T(8,128)} %get-tuple-element.16.mid_ref), custom_call_target="tpu_custom_call" | custom-call | tf_op jit(solution)/shard_map/down_sum/pallas_call | solution.py:411
  265.0 2.1 copy.20
  (28 shorter events, 0.3 us)
Async XLA Ops:
  6.5 111.9 %copy-start = (bf16[256,2048]{1,0:T(8,128)(2,1)S(1)}, bf16[256,2048]{1,0:T(8,128)(2,1)}, u32[]{:S(2)}) copy-start(bf16[256,2048]{1,0:T(8,128)(2,1)} %param.17) | copy-start | bytes 3145732
  6.5 188.5 %all-gather.4.cloned.1.call-start = ((), (), s32[]{:S(2)}) async-start(), calls=%async_computation | async-start | bytes 3604480 | tf_op jit(solution)/shard_map/all_gather | solution.py:466
  6.5 6.0 %copy-start.1 = (bf16[1408,256]{1,0:T(8,128)(2,1)S(1)}, bf16[1408,256]{1,0:T(8,128)(2,1)}, u32[]{:S(2)}) copy-start(bf16[1408,256]{1,0:T(8,128)(2,1)} %param.21) | copy-start | bytes 2162692
  8.8 6.5 %copy-start.3 = (bf16[768,256]{1,0:T(8,128)(2,1)S(1)}, bf16[768,256]{1,0:T(8,128)(2,1)}, u32[]{:S(2)}) copy-start(bf16[768,256]{1,0:T(8,128)(2,1)} %param.13) | copy-start | bytes 1179652
  9.9 196.0 %all-gather.6.cloned.1.call-start = ((), (), s32[]{:S(2)}) async-start(), calls=%async_computation.1 | async-start | bytes 3604480 | tf_op jit(solution)/shard_map/all_gather | solution.py:483
  11.0 25.9 %collective-permute-start = (bf16[256,1408]{1,0:T(8,128)(2,1)}, bf16[256,1408]{1,0:T(8,128)(2,1)S(1)}, u32[]{:S(2)}, u32[]{:S(2)}) collective-permute-start(bf16[256,1408]{1,0:T(8,128)(2,1)} %pad_maximum_fusion), channel_id=1, source_target_pairs={{0,4},{4,0},{8,12},{12,8},{16,20},{20,16},{24,28},{28,24},{1,5},{5... | collective-permute-start | bytes 2162696 | tf_op jit(solution)/shard_map/ppermute | solution.py:456
  13.3 5.0 %copy-start.5 = (f32[128]{0:T(128)S(1)}, f32[128]{0:T(128)}, u32[]{:S(2)}) copy-start(f32[128]{0:T(128)} %param.16) | copy-start | bytes 1540
  13.3 23.6 %collective-permute-start.1 = (bf16[704,256]{1,0:T(8,128)(2,1)}, bf16[704,256]{1,0:T(8,128)(2,1)}, u32[]{:S(2)}, u32[]{:S(2)}) collective-permute-start(bf16[704,256]{1,0:T(8,128)(2,1)} %get-tuple-element.28), channel_id=1, source_target_pairs={{0,4},{4,0},{8,12},{12,8},{16,20},{20,16},{24,28},{28,24},{1,5},{5... | collective-permute-start | bytes 1081352 | tf_op jit(solution)/shard_map/ppermute | solution.py:457
  15.2 3.4 %copy-start.6 = (f32[128]{0:T(128)S(1)}, f32[128]{0:T(128)}, u32[]{:S(2)}) copy-start(f32[128]{0:T(128)} %param.15) | copy-start | bytes 1540
  19.6 5.1 %copy-start.4 = (bf16[768,256]{1,0:T(8,128)(2,1)S(1)}, bf16[768,256]{1,0:T(8,128)(2,1)}, u32[]{:S(2)}) copy-start(bf16[768,256]{1,0:T(8,128)(2,1)} %param.14) | copy-start | bytes 1179652
  37.0 0.9 copy-start.2
  37.9 181.3 %all-gather.8.cloned.1.call-start = ((), (), s32[]{:S(2)}) async-start(), calls=%async_computation.2 | async-start | bytes 3604480 | tf_op jit(solution)/shard_map/all_gather | solution.py:486
Sparse Core Ops, SparseCore 0:
  10.1 74.1 all-gather.3
  85.8 57.6 all-gather.5
  145.1 57.7 all-gather.7
